TPU v7x, 32 devices: a whole 2x2x4 slice. The times are simulated.
32 devices in a mesh: ep: 8 (over z, core), tp: 4 (over y, x).
Axes of the slice: x: 2, y: 2, z: 4, core: 2. Of those that a mesh axis runs over, the one named last changes fastest.
Arguments:
- stream: bfloat16 [128, 4096], P('ep'), may hold values from -6 to 6
- previous_state: float32 [128, 128, 4096], P('ep', None, 'tp'), may hold values from -6 to 6
- mixer_norm_gain: float32 [4096], replicated, may hold values from 0.1 to 1.9
- query_matrix: bfloat16 [4096, 2048], P('ep'), may hold values from -0.09375 to 0.09375
- key_matrix: bfloat16 [4096, 2048], P('ep'), may hold values from -0.09375 to 0.09375
- value_matrix: bfloat16 [4096, 4096], P('ep', 'tp'), may hold values from -0.09375 to 0.09375
- output_gate_weight: bfloat16 [4096, 4096], P('ep', 'tp'), may hold values from -0.09375 to 0.09375
- decay_lower_factor: bfloat16 [4096, 64], replicated, may hold values from -0.09375 to 0.09375
- decay_upper_factor: bfloat16 [64, 2048], replicated, may hold values from -3 to 3
- forgetting_boost: float32 [128, 2048], P('ep'), may hold values from 0.02 to 1.5
- head_norm_gain: float32 [256], replicated, may hold values from 0.1 to 1.9
- output_matrix: bfloat16 [4096, 4096], P('tp'), may hold values from -0.1875 to 0.1875
- mixture_norm_gain: float32 [4096], replicated, may hold values from 0.1 to 1.9
- expert_gate_weight: bfloat16 [8, 1024, 4096], P('ep', 'tp'), may hold values from -0.09375 to 0.09375
- expert_up_weight: bfloat16 [8, 1024, 4096], P('ep', 'tp'), may hold values from -0.09375 to 0.09375
- expert_down_weight: bfloat16 [8, 1024, 4096], P('ep', None, 'tp'), may hold values from -0.375 to 0.375
- expert_index_table: int32 [128, 2], P('ep'), may hold values from 0 to 7, as said below
- expert_scores_within: float32 [128, 2], P('ep'), may hold values from -6 to 6
- group_probability: float32 [128], P('ep'), may hold values from 0.3 to 1
Outputs:
- new_stream: bfloat16 [128, 4096], P('ep', 'tp')
- new_state: float32 [128, 128, 4096], P('ep', None, 'tp')
Inputs may be any that keep to these rules, and one draw needn't show every extreme that they name: `expert_index_table`: the 2 experts of a sequence are distinct and lie in one group of 2 consecutive experts. Among the 16 sequences of one index of ep (aligned blocks of rows), each expert is named at most 8 times, and in every block some experts are named exactly 8 times.
All inputs are finite; a program needn't handle non-finite values.
Results may differ from a plain program's by a relative error of at most 0.02.
Values may be sent and summed in bfloat16 or wider, within the bound.
A program may use at most 128 MiB of HBM per device.

v0:
```python
import jax
import jax.numpy as jnp
from jax import lax
from jax.sharding import PartitionSpec as P

HEAD_TOTAL = 16
KEY_CHANNELS = 128
DV = 256
epsilon = 1e-06
forgetting_softness = 16.0


def rms_scaled(values, gain_vec):
    floats = values.astype(jnp.float32)
    scaled = floats * lax.rsqrt(jnp.mean(floats * floats, axis=-1, keepdims=True) + epsilon)
    return (scaled * gain_vec).astype(jnp.bfloat16)


def on_device(
    stream,
    previous_state,
    mixer_norm_gain,
    query_matrix,
    key_matrix,
    value_matrix,
    output_gate_weight,
    decay_lower_factor,
    decay_upper_factor,
    forgetting_boost,
    head_norm_gain,
    output_matrix,
    mixture_norm_gain,
    expert_gate_weight,
    expert_up_weight,
    expert_down_weight,
    expert_index_table,
    expert_scores_within,
    group_probability,
):
    seq_count, model_width = stream.shape
    value_local = previous_state.shape[2]
    head_count = max(1, value_local // DV)
    head_width = min(value_local, DV)
    tp_index = lax.axis_index("tp")
    leading_head = tp_index * value_local // DV
    value_start = tp_index * value_local % DV
    key_column_span = head_count * KEY_CHANNELS
    normed = rms_scaled(stream, mixer_norm_gain)
    own_query = lax.dynamic_slice_in_dim(
        query_matrix, leading_head * KEY_CHANNELS, key_column_span, 1
    )
    own_key = lax.dynamic_slice_in_dim(key_matrix, leading_head * KEY_CHANNELS, key_column_span, 1)
    spread = lax.all_to_all(normed, "ep", split_axis=1, concat_axis=0, tiled=True)
    joined = jnp.concatenate([own_query, own_key, value_matrix, output_gate_weight], axis=1)
    summed = lax.psum_scatter(
        jnp.dot(spread, joined, preferred_element_type=jnp.float32),
        "ep",
        scatter_dimension=0,
        tiled=True,
    )
    query_sum = summed[:, :key_column_span]
    key_sum = summed[:, key_column_span : 2 * key_column_span]
    value_sum = summed[:, 2 * key_column_span : 2 * key_column_span + value_local]
    gate_sum = summed[:, 2 * key_column_span + value_local :]
    queries = (query_sum * KEY_CHANNELS ** (-0.5)).astype(jnp.bfloat16)
    key_rows = key_sum.astype(jnp.bfloat16)
    value_rows = value_sum.astype(jnp.bfloat16)
    gate_rows = gate_sum.astype(jnp.bfloat16)
    low_rank = jnp.dot(normed, decay_lower_factor, preferred_element_type=jnp.float32).astype(
        jnp.bfloat16
    )
    local_expand_matrix = lax.dynamic_slice_in_dim(
        decay_upper_factor, leading_head * KEY_CHANNELS, key_column_span, 1
    )
    forgetting_logit = jnp.dot(low_rank, local_expand_matrix, preferred_element_type=jnp.float32)
    request_boost = lax.dynamic_slice_in_dim(
        forgetting_boost, leading_head * KEY_CHANNELS, key_column_span, 1
    )
    forgetting_lograte = jax.nn.log_sigmoid(forgetting_logit) / forgetting_softness - request_boost
    factor = (
        jnp.exp(forgetting_lograte)
        .reshape(seq_count, head_count, KEY_CHANNELS)
        .transpose(0, 2, 1)[..., None]
    )
    state_four = previous_state.reshape(seq_count, KEY_CHANNELS, head_count, head_width)
    key_part = (
        key_rows.astype(jnp.float32)
        .reshape(seq_count, head_count, KEY_CHANNELS)
        .transpose(0, 2, 1)[..., None]
    )
    value_part = value_rows.astype(jnp.float32).reshape(seq_count, 1, head_count, head_width)
    updated = factor * state_four + key_part * value_part
    query_part = (
        queries.astype(jnp.float32).reshape(seq_count, head_count, KEY_CHANNELS).transpose(0, 2, 1)
    )
    readout = jnp.einsum("skh,skhv->shv", query_part, updated, precision=lax.Precision.HIGHEST)
    square_sums = jnp.sum(readout * readout, axis=-1)
    norm_table = lax.dynamic_update_slice(
        jnp.zeros((seq_count, HEAD_TOTAL), jnp.float32), square_sums, (jnp.int32(0), leading_head)
    )
    totals = lax.psum(norm_table, "tp")
    own_totals = lax.dynamic_slice_in_dim(totals, leading_head, head_count, 1)
    mean_sq = own_totals[..., None] / DV
    own_gain = lax.dynamic_slice_in_dim(head_norm_gain, value_start, head_width, 0)
    gate_part = jax.nn.silu(
        gate_rows.astype(jnp.float32).reshape(seq_count, head_count, head_width)
    )
    gated_rows = (
        (readout * lax.rsqrt(mean_sq + epsilon) * own_gain * gate_part)
        .reshape(seq_count, value_local)
        .astype(jnp.bfloat16)
    )
    partial_out = jnp.dot(gated_rows, output_matrix, preferred_element_type=jnp.float32)
    mixer_sum = lax.psum(partial_out.astype(jnp.bfloat16), "tp").astype(jnp.float32)
    blended_tokens = (stream.astype(jnp.float32) + mixer_sum).astype(jnp.bfloat16)
    normed_two = rms_scaled(blended_tokens, mixture_norm_gain)
    ep_count = lax.axis_size("ep")
    local_experts = expert_gate_weight.shape[0]
    experts_all = ep_count * local_experts
    route_count = expert_index_table.shape[1]
    capacity = 2 * seq_count * route_count // experts_all
    slot_count = experts_all * capacity
    flat_ids = expert_index_table.reshape(seq_count * route_count)
    one_hot = (flat_ids[:, None] == jnp.arange(experts_all, dtype=jnp.int32)[None, :]).astype(
        jnp.int32
    )
    rank_in = jnp.sum(one_hot * (jnp.cumsum(one_hot, axis=0) - 1), axis=1)
    place_lookup = flat_ids * capacity + rank_in
    placing = (place_lookup[:, None] == jnp.arange(slot_count, dtype=jnp.int32)[None, :]).astype(
        jnp.float32
    )
    placing = placing.reshape(seq_count, route_count, slot_count)
    logit_exp = jnp.exp(expert_scores_within)
    weights = logit_exp / jnp.sum(logit_exp, axis=-1, keepdims=True) * group_probability[:, None]
    combine = jnp.einsum("sk,skc->sc", weights, placing, precision=lax.Precision.HIGHEST)
    dispatch = jnp.sum(placing, axis=1).astype(jnp.bfloat16)
    outgoing = jnp.einsum("sc,sd->cd", dispatch, normed_two, preferred_element_type=jnp.float32)
    outgoing = outgoing.astype(jnp.bfloat16).reshape(experts_all, capacity, model_width)
    width_local = expert_down_weight.shape[2]
    arrived = lax.all_to_all(outgoing, "ep", split_axis=0, concat_axis=0, tiled=True)
    held_slots = arrived.shape[1]
    grouped = arrived.reshape(ep_count, local_experts, held_slots, model_width)
    gate_pre = jnp.einsum(
        "sxcd,xfd->sxcf", grouped, expert_gate_weight, preferred_element_type=jnp.float32
    )
    up_pre = jnp.einsum(
        "sxcd,xfd->sxcf", grouped, expert_up_weight, preferred_element_type=jnp.float32
    )
    hidden = (jax.nn.silu(gate_pre) * up_pre).astype(jnp.bfloat16)
    outputs = jnp.einsum(
        "sxcf,xfd->sxcd",
        lax.all_gather(hidden, "tp", axis=3, tiled=True),
        expert_down_weight,
        preferred_element_type=jnp.float32,
    )
    ready_rows = outputs.astype(jnp.bfloat16).reshape(
        ep_count * local_experts, held_slots, width_local
    )
    returned = lax.all_to_all(ready_rows, "ep", split_axis=0, concat_axis=0, tiled=True)
    mixture = jnp.dot(
        combine,
        returned.reshape(slot_count, width_local).astype(jnp.float32),
        precision=lax.Precision.HIGHEST,
    )
    own_mixed = lax.dynamic_slice_in_dim(blended_tokens, tp_index * width_local, width_local, 1)
    new_stream = (own_mixed.astype(jnp.float32) + mixture).astype(jnp.bfloat16)
    return (new_stream, updated.reshape(seq_count, KEY_CHANNELS, value_local))


def solution(mesh):
    placed = (
        P("ep", None),
        P("ep", None, "tp"),
        P(),
        P("ep", None),
        P("ep", None),
        P("ep", "tp"),
        P("ep", "tp"),
        P(),
        P(),
        P("ep", None),
        P(),
        P("tp", None),
        P(),
        P("ep", "tp", None),
        P("ep", "tp", None),
        P("ep", None, "tp"),
        P("ep", None),
        P("ep", None),
        P("ep"),
    )
    return jax.shard_map(
        on_device,
        mesh=mesh,
        in_specs=placed,
        out_specs=(P("ep", "tp"), P("ep", None, "tp")),
        check_vma=False,
    )
```

profile of v0, /device:TPU:1, one launch (start us, length us, event | category | flops | bytes accessed | tf_op | source)
XLA Modules:
  0.0 207.3 jit_solution(5548687518825373681)
XLA Ops:
  7.2 0.0 copy-start
  7.2 1.2 fusion.36
  8.4 1.0 fusion.38
  9.4 0.7 copy.61
  10.1 6.4 %all-to-all-start = ((bf16[16,8,512]{2,0,1:T(8,128)(2,1)}), bf16[16,8,512]{2,0,1:T(8,128)(2,1)S(1)}, u32[]{:S(2)}, u32[]{:S(2)}) async-start(bf16[16,8,512]{2,0,1:T(8,128)(2,1)} %bitcast.84), calls=%async_computation | async-start | bytes 262144 | tf_op jit(solution)/shard_map/all_to_all | solution.py:53
  16.4 0.0 reduce-scatter.2.cloned.1.call-start
  16.4 1.3 constant_dynamic-slice_fusion
  17.7 4.5 %all-to-all-done = bf16[16,8,512]{2,0,1:T(8,128)(2,1)S(1)} async-done(((bf16[16,8,512]{2,0,1:T(8,128)(2,1)}), bf16[16,8,512]{2,0,1:T(8,128)(2,1)S(1)}, u32[]{:S(2)}, u32[]{:S(2)}) %all-to-all-start) | async-done | bytes 131104 | tf_op jit(solution)/shard_map/all_to_all | solution.py:53
  22.2 3.3 %fusion.3 = f32[128,3072]{1,0:T(8,128)} fusion(bf16[128,512]{1,0:T(8,128)(2,1)S(1)} %bitcast.90, bf16[512,1024]{1,0:T(8,128)(2,1)} %param.25, bf16[512,1024]{1,0:T(8,128)(2,1)} %param.24, bf16[512,512]{1,0:T(8,128)(2,1)S(1)} %get-tuple-element.6, bf16[512,512]{1,0:T(8,128)(2,1)S(1)} %get-tuple-element.7), kind=kOutput, calls=%fused_computation.7 | convolution fusion | flops 415236096 | bytes 4849664 | tf_op jit(solution)/shard_map/dot_general | solution.py:56
  25.5 0.0 reduce-scatter.2.cloned.1.call-update
  25.5 0.0 all-reduce.2.cloned.1.call-start
  25.6 0.0 copy-done.5
  25.6 0.1 copy.42
  25.7 0.1 eq.32
  25.8 0.1 fusion.60
  25.8 0.1 reduce_window_sum.11
  25.9 0.2 select_reduce_fusion
  26.1 0.1 reduce_sum.60
  26.2 0.1 copy.43
  26.3 10.6 %reshape.119 = f32[16,128,4,256]{3,2,1,0:T(4,128)} reshape(f32[16,128,1024]{2,1,0:T(8,128)} %param.20) | data formatting | bytes 16777216 | tf_op jit(solution)/shard_map/reshape | solution.py:85
  36.9 0.0 copy-done.3
  36.9 1.3 fusion.53
  38.2 0.4 copy.40
  38.6 17.5 %reduce-scatter.2.cloned.1.call-done = f32[16,3072]{1,0:T(8,128)} async-done(((f32[128,3072]{1,0:T(8,128)}), f32[16,3072]{1,0:T(8,128)}) %reduce-scatter.2.cloned.1.call-update) | async-done | bytes 196624 | tf_op jit(solution)/shard_map/reduce_scatter | solution.py:55
  56.1 0.9 convert.8
  57.1 1.4 copy.41
  58.6 0.8 fusion.54
  59.4 6.4 %multiply_add_fusion.1 = f32[16,128,4,256]{3,2,1,0:T(4,128)S(1)} fusion(f32[16,128,4,256]{3,2,1,0:T(4,128)} %reshape.119, f32[16,4,256]{2,1,0:T(4,128)S(1)} %mul.156, f32[16,128,4]{2,1,0:T(8,128)} %copy.41, f32[16,128,4]{2,1,0:T(8,128)S(1)} %copy.40), kind=kLoop, calls=%fused_computation.3 | loop fusion | flops 6291456 | bytes 16908288 | tf_op jit(solution)/shard_map/add | solution.py:92
  65.8 0.0 copy-start.6
  65.8 3.4 %fusion = f32[16,4,1,256]{3,2,1,0:T(1,128)S(1)} fusion(f32[16,128,4,256]{3,2,1,0:T(4,128)S(1)} %multiply_add_fusion.1, bf16[16,128,4,1]{1,2,0,3:T(4,128)(2,1)S(1)} %bitcast.87), kind=kOutput, calls=%fused_computation | convolution fusion | flops 25165824 | bytes 8470528 | tf_op jit(solution)/shard_map/skh,skhv->shv/dot_general | solution.py:96
  69.2 0.1 fusion.46
  69.3 0.2 dynamic_update_slice.3
  69.5 8.3 %psum.14 = f32[16,16]{1,0:T(8,128)S(1)} all-reduce(f32[16,16]{1,0:T(8,128)S(1)} %dynamic_update_slice.3), channel_id=1, replica_groups=mesh['ep'=8,'tp'=4] {'tp'}, use_global_device_ids=true, to_apply=%region_3.4 | all-reduce | flops 256 | bytes 2048 | tf_op jit(solution)/shard_map/psum | solution.py:101
  77.8 0.1 add_rsqrt_fusion
  77.9 0.0 copy-done.6
  77.9 0.1 fusion.49
  78.0 0.0 copy-start.2
  78.0 0.0 copy-start.4
  78.0 0.0 copy-start.7
  78.0 0.0 copy-start.8
  78.0 5.3 %convolution_convert_fusion.1 = bf16[16,4096]{1,0:T(8,128)(2,1)} fusion(bf16[16,1024]{1,0:T(8,128)(2,1)S(1)} %bitcast.86, bf16[1024,4096]{1,0:T(8,128)(2,1)} %param.30), kind=kOutput, calls=%fused_computation.6 | convolution fusion | flops 134283264 | bytes 8552448 | tf_op jit(solution)/shard_map/dot_general | solution.py:113
  83.4 0.0 all-reduce.2.cloned.1.call-update
  83.4 0.1 convert_reduce_fusion
  83.5 43.3 %all-reduce.2.cloned.1.call-done = bf16[16,4096]{1,0:T(8,128)(2,1)} async-done(((bf16[16,4096]{1,0:T(8,128)(2,1)}), bf16[16,4096]{1,0:T(8,128)(2,1)}) %all-reduce.2.cloned.1.call-update) | async-done | bytes 131088 | tf_op jit(solution)/shard_map/psum | solution.py:114
  126.8 1.1 fusion.33
  127.9 1.2 fusion.2
  129.0 5.7 %all-to-all-start.1 = ((bf16[8,8,4096]{2,1,0:T(8,128)(2,1)}), bf16[8,8,4096]{2,1,0:T(8,128)(2,1)}, u32[]{:S(2)}, u32[]{:S(2)}) async-start(bf16[8,8,4096]{2,1,0:T(8,128)(2,1)} %fusion.2), calls=%async_computation.2 | async-start | bytes 1048576 | tf_op jit(solution)/shard_map/all_to_all | solution.py:140
  134.7 0.0 copy-done.7
  134.8 0.1 copy.47
  134.8 4.5 %mul.153 = f32[16,128,4,256]{3,2,1,0:T(4,128)} broadcast(f32[16,128,4]{2,1,0:T(8,128)S(1)} %copy.40), dimensions={0,1,2} | broadcast | bytes 8421376 | tf_op jit(solution)/shard_map/mul | solution.py:92
  139.4 10.8 %mul.178 = f32[16,128,1024]{2,1,0:T(8,128)} reshape(f32[16,128,4,256]{3,2,1,0:T(4,128)} %mul.153) | data formatting | bytes 16777216 | tf_op jit(solution)/shard_map/mul | solution.py:92
  150.2 0.1 iota_compare_fusion
  150.3 0.2 fusion.58
  150.5 4.6 %mul.155 = f32[16,128,4,256]{3,2,1,0:T(4,128)} broadcast(f32[16,128,4]{2,1,0:T(8,128)S(1)} %copy-done.1), dimensions={0,1,2} | broadcast | bytes 8421376 | tf_op jit(solution)/shard_map/mul | solution.py:92
  155.1 10.7 %mul.180 = f32[16,128,1024]{2,1,0:T(8,128)} reshape(f32[16,128,4,256]{3,2,1,0:T(4,128)} %mul.155) | data formatting | bytes 16777216 | tf_op jit(solution)/shard_map/mul | solution.py:92
  165.8 0.0 all-to-all-done.1
  165.8 2.5 %fusion.20 = f32[8,1,8,256]{3,2,0,1:T(8,128)S(1)} fusion(bf16[8,8,4096]{2,1,0:T(8,128)(2,1)} %all-to-all-done.1, bf16[1,256,4096]{2,1,0:T(8,128)(2,1)} %param.32), kind=kOutput, calls=%fused_computation.23 | convolution fusion | flops 134217728 | bytes 2686976 | tf_op jit(solution)/shard_map/sxcd,xfd->sxcf/dot_general | solution.py:143
  168.3 2.5 %fusion.29 = bf16[8,1,8,256]{3,2,0,1:T(8,128)(2,1)S(1)} fusion(bf16[8,8,4096]{2,1,0:T(8,128)(2,1)} %all-to-all-done.1, bf16[1,256,4096]{2,1,0:T(8,128)(2,1)} %param.33, f32[8,1,8,256]{3,2,0,1:T(8,128)S(1)} %fusion.20), kind=kOutput, calls=%fused_computation.26 | convolution fusion | flops 134316032 | bytes 2719744 | tf_op jit(solution)/shard_map/sxcd,xfd->sxcf/dot_general | solution.py:146
  170.9 6.9 %all_gather.3 = bf16[8,1,8,1024]{3,2,0,1:T(8,128)(2,1)S(1)} all-gather(bf16[8,1,8,256]{3,2,0,1:T(8,128)(2,1)S(1)} %fusion.29), channel_id=1, replica_groups=mesh['ep'=8,'tp'=4] {'tp'}, dimensions={3}, use_global_device_ids=true | all-gather | bytes 163840 | tf_op jit(solution)/shard_map/all_gather | solution.py:152
  177.8 1.1 fusion.17
  178.9 7.1 %all-to-all-start.2 = ((bf16[8,8,1024]{2,1,0:T(8,128)(2,1)}), bf16[8,8,1024]{2,1,0:T(8,128)(2,1)S(1)}, u32[]{:S(2)}, u32[]{:S(2)}) async-start(bf16[8,8,1024]{2,1,0:T(8,128)(2,1)} %fusion.17), calls=%async_computation.3 | async-start | bytes 262144 | tf_op jit(solution)/shard_map/all_to_all | solution.py:159
  186.0 13.6 %multiply_add_fusion = f32[16,128,1024]{2,1,0:T(8,128)} fusion(f32[16,128,1024]{2,1,0:T(8,128)} %mul.180, f32[16,128,1024]{2,1,0:T(8,128)} %mul.178, f32[16,128,1024]{2,1,0:T(8,128)} %param.20, f32[16,1024]{1,0:T(8,128)S(1)} %get-tuple-element.4), kind=kLoop, calls=%fused_computation.2 | loop fusion | flops 6291456 | bytes 33619968 | tf_op jit(solution)/shard_map/add | solution.py:92
  199.6 0.0 all-to-all-done.2
  199.6 0.8 fusion.32
  (22 shorter events, 0.2 us)
Async XLA Ops:
  7.2 170.6 %copy-start = (bf16[1,1024,1024]{2,1,0:T(8,128)(2,1)S(1)}, bf16[1,1024,1024]{2,1,0:T(8,128)(2,1)}, u32[]{:S(2)}) copy-start(bf16[1,1024,1024]{2,1,0:T(8,128)(2,1)} %param.34) | copy-start | bytes 6291460
  10.1 12.1 %all-to-all-start = ((bf16[16,8,512]{2,0,1:T(8,128)(2,1)}), bf16[16,8,512]{2,0,1:T(8,128)(2,1)S(1)}, u32[]{:S(2)}, u32[]{:S(2)}) async-start(bf16[16,8,512]{2,0,1:T(8,128)(2,1)} %bitcast.84), calls=%async_computation | async-start | bytes 262144 | tf_op jit(solution)/shard_map/all_to_all | solution.py:53
  16.4 39.6 %reduce-scatter.2.cloned.1.call-start = ((), (), s32[]{:S(2)}) async-start(), calls=%async_computation.4 | async-start | bytes 1769472 | tf_op jit(solution)/shard_map/reduce_scatter | solution.py:55
  22.2 3.4 %copy-start.5 = (s32[16,2]{0,1:T(2,128)S(1)}, s32[16,2]{0,1:T(2,128)}, u32[]{:S(2)}) copy-start(s32[16,2]{0,1:T(2,128)} %param.35) | copy-start | bytes 388
  25.5 101.2 %all-reduce.2.cloned.1.call-start = ((), (), s32[]{:S(2)}) async-start(), calls=%async_computation.5 | async-start | bytes 262144 | tf_op jit(solution)/shard_map/psum | solution.py:114
  26.3 10.6 %copy-start.3 = (bf16[4096,64]{0,1:T(8,128)(2,1)S(1)}, bf16[4096,64]{0,1:T(8,128)(2,1)}, u32[]{:S(2)}) copy-start(bf16[4096,64]{0,1:T(8,128)(2,1)} %param.26) | copy-start | bytes 1572868
  65.8 12.1 %copy-start.6 = (f32[256]{0:T(256)S(1)}, f32[256]{0:T(256)}, u32[]{:S(2)}) copy-start(f32[256]{0:T(256)} %param.29) | copy-start | bytes 3076
  78.0 48.8 %copy-start.2 = (bf16[16,4096]{1,0:T(8,128)(2,1)S(1)}, bf16[16,4096]{1,0:T(8,128)(2,1)}, u32[]{:S(2)}) copy-start(bf16[16,4096]{1,0:T(8,128)(2,1)} %param.19) | copy-start | bytes 393220
  78.0 49.8 %copy-start.4 = (f32[4096]{0:T(1024)S(1)}, f32[4096]{0:T(1024)}, u32[]{:S(2)}) copy-start(f32[4096]{0:T(1024)} %param.31) | copy-start | bytes 49156
  78.0 56.7 %copy-start.7 = (f32[16,2]{0,1:T(2,128)S(1)}, f32[16,2]{0,1:T(2,128)}, u32[]{:S(2)}) copy-start(f32[16,2]{0,1:T(2,128)} %param.36) | copy-start | bytes 388
  78.0 56.7 %copy-start.8 = (f32[16]{0:T(128)S(1)}, f32[16]{0:T(128)}, u32[]{:S(2)}) copy-start(f32[16]{0:T(128)} %param.37) | copy-start | bytes 196
  129.0 36.8 %all-to-all-start.1 = ((bf16[8,8,4096]{2,1,0:T(8,128)(2,1)}), bf16[8,8,4096]{2,1,0:T(8,128)(2,1)}, u32[]{:S(2)}, u32[]{:S(2)}) async-start(bf16[8,8,4096]{2,1,0:T(8,128)(2,1)} %fusion.2), calls=%async_computation.2 | async-start | bytes 1048576 | tf_op jit(solution)/shard_map/all_to_all | solution.py:140
  139.4 11.1 %copy-start.1 = (f32[16,128,4]{2,1,0:T(8,128)S(1)}, f32[16,128,4]{2,1,0:T(8,128)}, u32[]{:S(2)}) copy-start(f32[16,128,4]{2,1,0:T(8,128)} %copy.41) | copy-start | bytes 98308
  178.9 20.7 %all-to-all-start.2 = ((bf16[8,8,1024]{2,1,0:T(8,128)(2,1)}), bf16[8,8,1024]{2,1,0:T(8,128)(2,1)S(1)}, u32[]{:S(2)}, u32[]{:S(2)}) async-start(bf16[8,8,1024]{2,1,0:T(8,128)(2,1)} %fusion.17), calls=%async_computation.3 | async-start | bytes 262144 | tf_op jit(solution)/shard_map/all_to_all | solution.py:159
Sparse Core Ops, SparseCore 0:
  25.7 30.3 reduce-scatter.1
  83.5 43.2 all-reduce.1
where the time goes:
time: 209 us; the launch traced here: 207 us
  waiting for transfers between devices  65.4 us (31%)
  local copies, waits for them, and re-layouts  45.8 us (22%)
  other arithmetic  25.8 us (12%)
  matrix products  21.6 us (10%)
  starting transfers between devices  19.2 us (9%)
  blocking collectives  15.2 us (7%)
  between operations  14.3 us (7%)
    psum x1, waiting for transfers between devices, on_device(): lax.psum(partial_out.astype(jnp.bfloat16), 'tp').astype(jnp.float32)  43.3 us
    mul x5, local copies, waits for them, and re-layouts, on_device(): updated = factor * state_four + key_part * value_part  30.7 us
    add x2, other arithmetic, on_device(): updated = factor * state_four + key_part * value_part  20 us
    reduce_scatter x1, waiting for transfers between devices, on_device(): lax.psum_scatter(jnp.dot(spread, joined, preferred_element_type=jnp.float...  17.5 us
    reshape x1, local copies, waits for them, and re-layouts, on_device(): previous_state.reshape(seq_count, KEY_CHANNELS, head_count, head_width)  10.6 us
    psum x1, blocking collectives, on_device(): totals = lax.psum(norm_table, 'tp')  8.28 us
    all_to_all x1, starting transfers between devices, on_device(): lax.all_to_all(ready_rows, 'ep', split_axis=0, concat_axis=0, tiled=True)  7.12 us
    all_gather x1, blocking collectives, on_device(): lax.all_gather(hidden, 'tp', axis=3, tiled=True)  6.91 us
  transfers between devices with their start and end apart: 5, of which 3 were waited for; matrix products, arithmetic and copies ran while one was open for 28% of the time, Pallas kernels for 0%

commit v1 on v0

--- a/solution.py
+++ b/solution.py
@@ -8,6 +8,12 @@
 DV = 256
 epsilon = 1e-06
 forgetting_softness = 16.0
+
+
+def summed_here(x, mesh_axis):
+    pieces = lax.all_gather(x, mesh_axis, axis=0, tiled=False)
+    acc = pieces.sum(axis=0)
+    return acc
 
 
 def rms_scaled(values, gain_vec):
@@ -111,7 +117,7 @@
         .astype(jnp.bfloat16)
     )
     partial_out = jnp.dot(gated_rows, output_matrix, preferred_element_type=jnp.float32)
-    mixer_sum = lax.psum(partial_out.astype(jnp.bfloat16), "tp").astype(jnp.float32)
+    mixer_sum = summed_here(partial_out.astype(jnp.bfloat16), "tp").astype(jnp.float32)
     blended_tokens = (stream.astype(jnp.float32) + mixer_sum).astype(jnp.bfloat16)
     normed_two = rms_scaled(blended_tokens, mixture_norm_gain)
     ep_count = lax.axis_size("ep")

time: 209 us -> 180 us (0.86)
  waiting for transfers between devices: 65.4 us -> 22 us
  blocking collectives: 15.2 us -> 23.1 us
  starting transfers between devices: 19.2 us -> 25.1 us
    psum x1 -> x0, waiting for transfers between devices: 43.3 us -> none  [on_device(): lax.psum(partial_out.astype(jnp.bfloat16), 'tp').astype(jnp.float32)]
    all_gather x0 -> x1, blocking collectives: none -> 8.03 us  [summed_here(): pieces = lax.all_gather(x, mesh_axis, axis=0, tiled=False)]
    all_to_all x1, starting transfers between devices: 5.72 us -> 11.6 us  [on_device(): lax.all_to_all(outgoing, 'ep', split_axis=0, concat_axis=0, tiled=True)]
  transfers between devices with their start and end apart: 5 -> 4, of which waited for: 3 -> 2; matrix products, arithmetic and copies ran while one was open for 28% -> 33% of each run, Pallas kernels for 0% -> 0%
where the time goes in v1:
time: 180 us; the launch traced here: 179 us
  local copies, waits for them, and re-layouts  45.8 us (25%)
  other arithmetic  27.6 us (15%)
  starting transfers between devices  25.1 us (14%)
  blocking collectives  23.1 us (13%)
  waiting for transfers between devices  22 us (12%)
  matrix products  20.9 us (12%)
  between operations  14.3 us (8%)
    mul x5, local copies, waits for them, and re-layouts, on_device(): updated = factor * state_four + key_part * value_part  30.7 us
    add x2, other arithmetic, on_device(): updated = factor * state_four + key_part * value_part  20 us
    reduce_scatter x1, waiting for transfers between devices, on_device(): lax.psum_scatter(jnp.dot(spread, joined, preferred_element_type=jnp.float...  17.5 us
    all_to_all x1, starting transfers between devices, on_device(): lax.all_to_all(outgoing, 'ep', split_axis=0, concat_axis=0, tiled=True)  11.6 us
    reshape x1, local copies, waits for them, and re-layouts, on_device(): previous_state.reshape(seq_count, KEY_CHANNELS, head_count, head_width)  10.6 us
    psum x1, blocking collectives, on_device(): totals = lax.psum(norm_table, 'tp')  8.25 us
    all_gather x1, blocking collectives, summed_here(): pieces = lax.all_gather(x, mesh_axis, axis=0, tiled=False)  8.03 us
    all_to_all x1, starting transfers between devices, on_device(): lax.all_to_all(ready_rows, 'ep', split_axis=0, concat_axis=0, tiled=True)  7.15 us
  transfers between devices with their start and end apart: 4, of which 2 were waited for; matrix products, arithmetic and copies ran while one was open for 33% of the time, Pallas kernels for 0%

profile of v1, /device:TPU:1, one launch (start us, length us, event | category | flops | bytes accessed | tf_op | source)
XLA Modules:
  0.0 178.9 jit_solution(7231097450512045417)
XLA Ops:
  7.2 0.0 copy-start
  7.2 1.2 fusion.36
  8.4 1.0 fusion.38
  9.4 0.7 copy.61
  10.1 6.4 %all-to-all-start = ((bf16[16,8,512]{2,0,1:T(8,128)(2,1)}), bf16[16,8,512]{2,0,1:T(8,128)(2,1)S(1)}, u32[]{:S(2)}, u32[]{:S(2)}) async-start(bf16[16,8,512]{2,0,1:T(8,128)(2,1)} %bitcast.85), calls=%async_computation | async-start | bytes 262144 | tf_op jit(solution)/shard_map/all_to_all | solution.py:59
  16.4 0.0 reduce-scatter.2.cloned.1.call-start
  16.4 1.3 constant_dynamic-slice_fusion
  17.7 4.5 %all-to-all-done = bf16[16,8,512]{2,0,1:T(8,128)(2,1)S(1)} async-done(((bf16[16,8,512]{2,0,1:T(8,128)(2,1)}), bf16[16,8,512]{2,0,1:T(8,128)(2,1)S(1)}, u32[]{:S(2)}, u32[]{:S(2)}) %all-to-all-start) | async-done | bytes 131104 | tf_op jit(solution)/shard_map/all_to_all | solution.py:59
  22.2 3.3 %fusion.3 = f32[128,3072]{1,0:T(8,128)} fusion(bf16[128,512]{1,0:T(8,128)(2,1)S(1)} %bitcast.92, bf16[512,1024]{1,0:T(8,128)(2,1)} %param.25, bf16[512,1024]{1,0:T(8,128)(2,1)} %param.24, bf16[512,512]{1,0:T(8,128)(2,1)S(1)} %get-tuple-element.6, bf16[512,512]{1,0:T(8,128)(2,1)S(1)} %get-tuple-element.7), kind=kOutput, calls=%fused_computation.7 | convolution fusion | flops 415236096 | bytes 4849664 | tf_op jit(solution)/shard_map/dot_general | solution.py:62
  25.5 0.0 reduce-scatter.2.cloned.1.call-update
  25.5 0.0 copy-done.5
  25.5 0.1 copy.42
  25.6 0.1 eq.32
  25.7 0.1 fusion.60
  25.8 0.1 reduce_window_sum.11
  25.9 0.2 select_reduce_fusion
  26.0 0.1 reduce_sum.73
  26.1 0.1 copy.43
  26.2 10.6 %reshape.119 = f32[16,128,4,256]{3,2,1,0:T(4,128)} reshape(f32[16,128,1024]{2,1,0:T(8,128)} %param.20) | data formatting | bytes 16777216 | tf_op jit(solution)/shard_map/reshape | solution.py:91
  36.8 0.0 copy-done.3
  36.8 1.3 fusion.53
  38.1 0.4 copy.40
  38.5 0.1 convert_reduce_fusion
  38.6 17.5 %reduce-scatter.2.cloned.1.call-done = f32[16,3072]{1,0:T(8,128)} async-done(((f32[128,3072]{1,0:T(8,128)}), f32[16,3072]{1,0:T(8,128)}) %reduce-scatter.2.cloned.1.call-update) | async-done | bytes 196624 | tf_op jit(solution)/shard_map/reduce_scatter | solution.py:61
  56.1 0.9 convert.9
  57.1 1.4 copy.41
  58.6 0.8 fusion.54
  59.4 6.4 %multiply_add_fusion.1 = f32[16,128,4,256]{3,2,1,0:T(4,128)S(1)} fusion(f32[16,128,4,256]{3,2,1,0:T(4,128)} %reshape.119, f32[16,4,256]{2,1,0:T(4,128)S(1)} %mul.156, f32[16,128,4]{2,1,0:T(8,128)} %copy.41, f32[16,128,4]{2,1,0:T(8,128)S(1)} %copy.40), kind=kLoop, calls=%fused_computation.3 | loop fusion | flops 6291456 | bytes 16908288 | tf_op jit(solution)/shard_map/add | solution.py:98
  65.8 0.0 copy-start.6
  65.8 3.4 %fusion = f32[16,4,1,256]{3,2,1,0:T(1,128)S(1)} fusion(f32[16,128,4,256]{3,2,1,0:T(4,128)S(1)} %multiply_add_fusion.1, bf16[16,128,4,1]{1,2,0,3:T(4,128)(2,1)S(1)} %bitcast.89), kind=kOutput, calls=%fused_computation | convolution fusion | flops 25165824 | bytes 8470528 | tf_op jit(solution)/shard_map/skh,skhv->shv/dot_general | solution.py:102
  69.2 0.1 fusion.46
  69.3 0.2 dynamic_update_slice.3
  69.5 8.3 %psum.7 = f32[16,16]{1,0:T(8,128)S(1)} all-reduce(f32[16,16]{1,0:T(8,128)S(1)} %dynamic_update_slice.3), channel_id=1, replica_groups=mesh['ep'=8,'tp'=4] {'tp'}, use_global_device_ids=true, to_apply=%region_3.4 | all-reduce | flops 256 | bytes 2048 | tf_op jit(solution)/shard_map/psum | solution.py:107
  77.8 0.1 add_rsqrt_fusion
  77.9 0.0 copy-done.6
  77.9 0.1 fusion.49
  78.0 0.0 copy-start.2
  78.0 0.0 copy-start.4
  78.0 0.0 copy-start.7
  78.0 0.0 copy-start.8
  78.0 4.6 %convolution_convert_fusion.1 = bf16[16,4096]{1,0:T(8,128)(2,1)S(1)} fusion(bf16[16,1024]{1,0:T(8,128)(2,1)S(1)} %bitcast.88, bf16[1024,4096]{1,0:T(8,128)(2,1)} %param.30), kind=kOutput, calls=%fused_computation.6 | convolution fusion | flops 134283264 | bytes 8552448 | tf_op jit(solution)/shard_map/dot_general | solution.py:119
  82.7 8.0 %all-gather = bf16[64,4096]{1,0:T(8,128)(2,1)} all-gather(bf16[16,4096]{1,0:T(8,128)(2,1)S(1)} %convolution_convert_fusion.1), channel_id=2, replica_groups=mesh['ep'=8,'tp'=4] {'tp'}, dimensions={0}, use_global_device_ids=true | all-gather | bytes 655360 | tf_op jit(solution)/shard_map/all_gather | solution.py:14
  90.7 1.8 %reduce_sum.70 = bf16[16,4096]{1,0:T(8,128)(2,1)} reduce(bf16[4,16,4096]{2,1,0:T(8,128)(2,1)} %bitcast.86, bf16[]{:T(256)} %constant.69.clone.1), dimensions={0}, to_apply=%region_4.5 | reduce | flops 196608 | bytes 655362 | tf_op jit(solution)/shard_map/reduce_sum | solution.py:15
  92.5 0.0 copy-done.2
  92.5 1.1 fusion.33
  93.6 1.2 fusion.2
  94.7 11.6 %all-to-all-start.1 = ((bf16[8,8,4096]{2,1,0:T(8,128)(2,1)}), bf16[8,8,4096]{2,1,0:T(8,128)(2,1)}, u32[]{:S(2)}, u32[]{:S(2)}) async-start(bf16[8,8,4096]{2,1,0:T(8,128)(2,1)} %fusion.2), calls=%async_computation.2 | async-start | bytes 1048576 | tf_op jit(solution)/shard_map/all_to_all | solution.py:146
  106.4 0.0 copy-done.8
  106.4 0.1 copy.47
  106.5 4.5 %mul.153 = f32[16,128,4,256]{3,2,1,0:T(4,128)} broadcast(f32[16,128,4]{2,1,0:T(8,128)S(1)} %copy.40), dimensions={0,1,2} | broadcast | bytes 8421376 | tf_op jit(solution)/shard_map/mul | solution.py:98
  111.0 10.8 %mul.178 = f32[16,128,1024]{2,1,0:T(8,128)} reshape(f32[16,128,4,256]{3,2,1,0:T(4,128)} %mul.153) | data formatting | bytes 16777216 | tf_op jit(solution)/shard_map/mul | solution.py:98
  121.8 0.1 iota_compare_fusion
  121.9 0.2 fusion.58
  122.1 4.6 %mul.155 = f32[16,128,4,256]{3,2,1,0:T(4,128)} broadcast(f32[16,128,4]{2,1,0:T(8,128)S(1)} %copy-done.1), dimensions={0,1,2} | broadcast | bytes 8421376 | tf_op jit(solution)/shard_map/mul | solution.py:98
  126.7 10.7 %mul.180 = f32[16,128,1024]{2,1,0:T(8,128)} reshape(f32[16,128,4,256]{3,2,1,0:T(4,128)} %mul.155) | data formatting | bytes 16777216 | tf_op jit(solution)/shard_map/mul | solution.py:98
  137.4 0.0 all-to-all-done.1
  137.4 2.5 %fusion.20 = f32[8,1,8,256]{3,2,0,1:T(8,128)S(1)} fusion(bf16[8,8,4096]{2,1,0:T(8,128)(2,1)} %all-to-all-done.1, bf16[1,256,4096]{2,1,0:T(8,128)(2,1)} %param.32), kind=kOutput, calls=%fused_computation.23 | convolution fusion | flops 134217728 | bytes 2686976 | tf_op jit(solution)/shard_map/sxcd,xfd->sxcf/dot_general | solution.py:149
  140.0 2.5 %fusion.29 = bf16[8,1,8,256]{3,2,0,1:T(8,128)(2,1)S(1)} fusion(bf16[8,8,4096]{2,1,0:T(8,128)(2,1)} %all-to-all-done.1, bf16[1,256,4096]{2,1,0:T(8,128)(2,1)} %param.33, f32[8,1,8,256]{3,2,0,1:T(8,128)S(1)} %fusion.20), kind=kOutput, calls=%fused_computation.26 | convolution fusion | flops 134316032 | bytes 2719744 | tf_op jit(solution)/shard_map/sxcd,xfd->sxcf/dot_general | solution.py:152
  142.5 6.8 %all_gather.11 = bf16[8,1,8,1024]{3,2,0,1:T(8,128)(2,1)S(1)} all-gather(bf16[8,1,8,256]{3,2,0,1:T(8,128)(2,1)S(1)} %fusion.29), channel_id=1, replica_groups=mesh['ep'=8,'tp'=4] {'tp'}, dimensions={3}, use_global_device_ids=true | all-gather | bytes 163840 | tf_op jit(solution)/shard_map/all_gather | solution.py:158
  149.3 1.1 fusion.17
  150.5 7.2 %all-to-all-start.2 = ((bf16[8,8,1024]{2,1,0:T(8,128)(2,1)}), bf16[8,8,1024]{2,1,0:T(8,128)(2,1)S(1)}, u32[]{:S(2)}, u32[]{:S(2)}) async-start(bf16[8,8,1024]{2,1,0:T(8,128)(2,1)} %fusion.17), calls=%async_computation.3 | async-start | bytes 262144 | tf_op jit(solution)/shard_map/all_to_all | solution.py:165
  157.6 13.6 %multiply_add_fusion = f32[16,128,1024]{2,1,0:T(8,128)} fusion(f32[16,128,1024]{2,1,0:T(8,128)} %mul.180, f32[16,128,1024]{2,1,0:T(8,128)} %mul.178, f32[16,128,1024]{2,1,0:T(8,128)} %param.20, f32[16,1024]{1,0:T(8,128)S(1)} %get-tuple-element.4), kind=kLoop, calls=%fused_computation.2 | loop fusion | flops 6291456 | bytes 33619968 | tf_op jit(solution)/shard_map/add | solution.py:98
  171.2 0.0 all-to-all-done.2
  171.2 0.8 fusion.32
  (21 shorter events, 0.2 us)
Async XLA Ops:
  7.2 142.2 %copy-start = (bf16[1,1024,1024]{2,1,0:T(8,128)(2,1)S(1)}, bf16[1,1024,1024]{2,1,0:T(8,128)(2,1)}, u32[]{:S(2)}) copy-start(bf16[1,1024,1024]{2,1,0:T(8,128)(2,1)} %param.34) | copy-start | bytes 6291460
  10.1 12.1 %all-to-all-start = ((bf16[16,8,512]{2,0,1:T(8,128)(2,1)}), bf16[16,8,512]{2,0,1:T(8,128)(2,1)S(1)}, u32[]{:S(2)}, u32[]{:S(2)}) async-start(bf16[16,8,512]{2,0,1:T(8,128)(2,1)} %bitcast.85), calls=%async_computation | async-start | bytes 262144 | tf_op jit(solution)/shard_map/all_to_all | solution.py:59
  16.4 39.6 %reduce-scatter.2.cloned.1.call-start = ((), (), s32[]{:S(2)}) async-start(), calls=%async_computation.4 | async-start | bytes 1769472 | tf_op jit(solution)/shard_map/reduce_scatter | solution.py:61
  22.2 3.3 %copy-start.5 = (s32[16,2]{0,1:T(2,128)S(1)}, s32[16,2]{0,1:T(2,128)}, u32[]{:S(2)}) copy-start(s32[16,2]{0,1:T(2,128)} %param.35) | copy-start | bytes 388
  26.2 10.6 %copy-start.3 = (bf16[4096,64]{0,1:T(8,128)(2,1)S(1)}, bf16[4096,64]{0,1:T(8,128)(2,1)}, u32[]{:S(2)}) copy-start(bf16[4096,64]{0,1:T(8,128)(2,1)} %param.26) | copy-start | bytes 1572868
  65.8 12.1 %copy-start.6 = (f32[256]{0:T(256)S(1)}, f32[256]{0:T(256)}, u32[]{:S(2)}) copy-start(f32[256]{0:T(256)} %param.29) | copy-start | bytes 3076
  78.0 14.5 %copy-start.2 = (bf16[16,4096]{1,0:T(8,128)(2,1)S(1)}, bf16[16,4096]{1,0:T(8,128)(2,1)}, u32[]{:S(2)}) copy-start(bf16[16,4096]{1,0:T(8,128)(2,1)} %param.19) | copy-start | bytes 393220
  78.0 15.6 %copy-start.4 = (f32[4096]{0:T(1024)S(1)}, f32[4096]{0:T(1024)}, u32[]{:S(2)}) copy-start(f32[4096]{0:T(1024)} %param.31) | copy-start | bytes 49156
  78.0 28.4 %copy-start.7 = (f32[16,2]{0,1:T(2,128)S(1)}, f32[16,2]{0,1:T(2,128)}, u32[]{:S(2)}) copy-start(f32[16,2]{0,1:T(2,128)} %param.36) | copy-start | bytes 388
  78.0 28.4 %copy-start.8 = (f32[16]{0:T(128)S(1)}, f32[16]{0:T(128)}, u32[]{:S(2)}) copy-start(f32[16]{0:T(128)} %param.37) | copy-start | bytes 196
  94.7 42.7 %all-to-all-start.1 = ((bf16[8,8,4096]{2,1,0:T(8,128)(2,1)}), bf16[8,8,4096]{2,1,0:T(8,128)(2,1)}, u32[]{:S(2)}, u32[]{:S(2)}) async-start(bf16[8,8,4096]{2,1,0:T(8,128)(2,1)} %fusion.2), calls=%async_computation.2 | async-start | bytes 1048576 | tf_op jit(solution)/shard_map/all_to_all | solution.py:146
  111.0 11.1 %copy-start.1 = (f32[16,128,4]{2,1,0:T(8,128)S(1)}, f32[16,128,4]{2,1,0:T(8,128)}, u32[]{:S(2)}) copy-start(f32[16,128,4]{2,1,0:T(8,128)} %copy.41) | copy-start | bytes 98308
  150.5 20.8 %all-to-all-start.2 = ((bf16[8,8,1024]{2,1,0:T(8,128)(2,1)}), bf16[8,8,1024]{2,1,0:T(8,128)(2,1)S(1)}, u32[]{:S(2)}, u32[]{:S(2)}) async-start(bf16[8,8,1024]{2,1,0:T(8,128)(2,1)} %fusion.17), calls=%async_computation.3 | async-start | bytes 262144 | tf_op jit(solution)/shard_map/all_to_all | solution.py:165
Sparse Core Ops, SparseCore 0:
  25.7 30.3 reduce-scatter.1
